TPU v7x, 32 devices: a whole 2x2x4 slice. The times are simulated.
32 devices in a mesh: sp: 4 (over z), fs: 4 (over y, x), tp: 2 (over core).
Axes of the slice: x: 2, y: 2, z: 4, core: 2. Of those that a mesh axis runs over, the one named last changes fastest.
Arguments:
- tokens: bfloat16 [4, 2048, 2048], P('fs', 'sp', 'tp'), may hold values from -6 to 6
- norm_gain: float32 [2048], replicated, may hold values from 0.1 to 1.9
- query_weight: bfloat16 [2048, 1024], P(('sp', 'fs'), 'tp'), may hold values from -0.125 to 0.125
- key_weight: bfloat16 [2048, 1024], P(('sp', 'fs'), 'tp'), may hold values from -0.125 to 0.125
- value_weight: bfloat16 [2048, 2048], P(('sp', 'fs'), 'tp'), may hold values from -0.125 to 0.125
- outgate_weight: bfloat16 [2048, 2048], P(('sp', 'fs'), 'tp'), may hold values from -0.125 to 0.125
- gate_weight: bfloat16 [2048, 2, 16], P(('sp', 'fs'), None, 'tp'), may hold values from -6 to 6
- forget_bias: float32 [16], P('tp')
- forget_shift: float32 [4, 16, 2048], P('fs', 'tp', 'sp'), may hold values from -1.5 to 0
- head_norm_gain: float32 [2048], P('tp'), may hold values from 0.1 to 1.9
- exit_weight: bfloat16 [2048, 2048], P(('sp', 'fs'), 'tp'), may hold values from -0.125 to 0.125
- entry_weight: bfloat16 [2048, 2048], P(('sp', 'fs'), 'tp'), may hold values from -0.125 to 0.125
- signal_weight: bfloat16 [2048, 2048], P(('sp', 'fs'), 'tp'), may hold values from -0.125 to 0.125
- conv_kernel: float32 [3, 2048], P(None, 'tp'), may hold values from -3.5 to 3.5
- merge_weight: bfloat16 [4096, 2048], P(('sp', 'fs'), 'tp'), may hold values from -0.09375 to 0.09375
Outputs:
- mixed: bfloat16 [4, 2048, 2048], P('fs', 'sp', 'tp')
All inputs are finite; a program needn't handle non-finite values.
Results may differ from a plain program's by a relative error of at most 0.017.
The roundings to bfloat16 on the way count: a program that leaves them out, or rounds other values in their place, can miss the bound.
Values may be sent and summed in bfloat16 or wider, within the bound.
A program may use at most 128 MiB of HBM per device.

v0:
```python
import jax
import jax.numpy as jnp
from jax import lax
from jax.sharding import PartitionSpec as P

DK = 64
DV = 128
BLOCK = 128
KERNEL = 3
EPSILON = 1e-06
EMPTY_LOG = -1e30
HIGHEST = lax.Precision.HIGHEST


def prefix(part, axis, combine, identity):
    place = lax.axis_index(axis)
    gathered = jax.tree.map(lambda a: lax.all_gather(a, axis), part)
    state = jax.tree.map(lambda a, e: jnp.zeros_like(a) + jnp.asarray(e, a.dtype), part, identity)

    def one(step, state):
        return combine(
            state, jax.tree.map(lambda a: lax.dynamic_index_in_dim(a, step, 0, False), gathered)
        )

    return lax.fori_loop(0, place, one, state)


def passed_along(value, axis, steps):
    count = lax.axis_size(axis)
    initial, last = (max(0, -steps), min(count, count - steps))
    return lax.ppermute(value, axis, [(source, source + steps) for source in range(initial, last)])


def combine(earlier, later):
    ceiling = jnp.maximum(later[2] + earlier[1], later[1])
    kept = jnp.exp(later[2] + earlier[1] - ceiling)
    added = jnp.exp(later[1] - ceiling)
    state = kept[..., None, None] * earlier[0] + added[..., None, None] * later[0]
    return (state, ceiling, earlier[2] + later[2])


def identity_state(heads):
    return (
        jnp.zeros((heads, DK, DV), jnp.float32),
        jnp.full((heads,), EMPTY_LOG, jnp.float32),
        jnp.zeros((heads,), jnp.float32),
    )


def add_product(left, piece):
    return jnp.dot(left, piece, preferred_element_type=jnp.float32)


def split_columns(total, stack):
    outputs = []
    offset = 0
    for weight in stack:
        outputs.append(total[:, offset : offset + weight.shape[1]])
        offset = offset + weight.shape[1]
    return outputs


def incoming_state(running):
    heads = running[1].shape[0]
    before = prefix((running[0], running[1], running[2]), "sp", combine, identity_state(heads))
    ceiling = jnp.maximum(before[1], before[2])
    shrink = jnp.exp(before[1] - ceiling)
    return (before[0] * shrink[:, None, None], ceiling, before[2])


def memory_states(keys, values, gates, forget_bias, forget_shift):
    count = gates.shape[0]
    heads = forget_bias.shape[0]
    blocks = count // BLOCK
    inputs = gates[:, :heads].reshape(blocks, BLOCK, heads)
    logs = jax.nn.log_sigmoid(gates[:, heads:] + forget_bias) + forget_shift[0].T
    cumulative = jnp.cumsum(logs.reshape(blocks, BLOCK, heads), axis=1)
    last = cumulative[:, -1]
    weight_logs = last[:, None, :] - cumulative + inputs
    peak = jnp.max(weight_logs, axis=1)
    coefficient_array = jnp.exp(weight_logs - peak[:, None, :])
    scaled = keys.reshape(blocks, BLOCK, heads, DK).astype(jnp.float32) * DK ** (-0.5)
    value_float = values.reshape(blocks, BLOCK, heads, DV).astype(jnp.float32)
    states = jnp.einsum(
        "csh,cshk,cshv->chkv", coefficient_array, scaled, value_float, precision=HIGHEST
    )
    running = identity_state(heads)
    prefixes = []
    for index in range(blocks):
        prefixes.append(running)
        running = combine(running, (states[index], peak[index], last[index]))
    leading_part = tuple((jnp.stack([item[member] for item in prefixes]) for member in range(3)))
    gate_apertures = combine(incoming_state(running), leading_part)
    return (gate_apertures, cumulative, inputs)


def memory_output(
    queries, keys, values, outgates, inputs, cumulative, gate_apertures, head_norm_gain
):
    blocks = cumulative.shape[0]
    heads = cumulative.shape[2]
    count = queries.shape[0]
    query_blocks = queries.reshape(blocks, BLOCK, heads, DK)
    key_blocks = keys.reshape(blocks, BLOCK, heads, DK)
    value_blocks = values.reshape(blocks, BLOCK, heads, DV)
    score_matrix = jnp.einsum(
        "cjhk,cshk->chjs", query_blocks, key_blocks, preferred_element_type=jnp.float32
    ) * DK ** (-0.5)
    cum_lanes = cumulative.transpose(0, 2, 1)
    input_lanes = inputs.transpose(0, 2, 1)
    causal = jnp.tril(jnp.ones((BLOCK, BLOCK), dtype=bool))
    decay = jnp.where(
        causal,
        cum_lanes[..., :, None] - cum_lanes[..., None, :] + input_lanes[..., None, :],
        -jnp.inf,
    )
    inter = cum_lanes + gate_apertures[1][..., None]
    ceiling = jnp.maximum(inter, jnp.max(decay, axis=-1))
    weighted = score_matrix * jnp.exp(decay - ceiling[..., None])
    numerator = jnp.einsum(
        "chjs,cshv->chjv",
        weighted.astype(jnp.bfloat16),
        value_blocks,
        preferred_element_type=jnp.float32,
    )
    query_float = query_blocks.astype(jnp.float32)
    carried = jnp.exp(inter - ceiling)
    numerator = numerator + carried[..., None] * jnp.einsum(
        "cjhk,chkv->chjv", query_float, gate_apertures[0], precision=HIGHEST
    )
    result = numerator * lax.rsqrt(
        jnp.mean(numerator * numerator, axis=-1, keepdims=True) + EPSILON
    )
    result = result.transpose(0, 2, 1, 3).reshape(count, heads * DV) * head_norm_gain
    return (result * jax.nn.sigmoid(outgates.astype(jnp.float32))).astype(jnp.bfloat16)


def local(
    tokens,
    norm_gain,
    query_weight,
    key_weight,
    value_weight,
    outgate_weight,
    gate_weight,
    forget_bias,
    forget_shift,
    head_norm_gain,
    exit_weight,
    entry_weight,
    signal_weight,
    conv_kernel,
    merge_weight,
):
    whole = lax.all_gather(tokens, "tp", axis=2, tiled=True)[0]
    count = whole.shape[0]
    flat = whole.astype(jnp.float32)
    normed = (
        flat * lax.rsqrt(jnp.mean(flat * flat, axis=-1, keepdims=True) + EPSILON) * norm_gain
    ).astype(jnp.bfloat16)
    gate_rows = gate_weight.reshape(gate_weight.shape[0], -1)
    state_stack = [key_weight, value_weight, gate_rows]
    other_stack = [query_weight, outgate_weight, exit_weight, entry_weight, signal_weight]
    stacked = jnp.concatenate(state_stack + other_stack, axis=1)
    total = add_product(normed, lax.all_gather(stacked, ("sp", "fs"), axis=0, tiled=True))
    columns = split_columns(total, state_stack + other_stack)
    keys = columns[0].astype(jnp.bfloat16)
    values = columns[1].astype(jnp.bfloat16)
    gate_apertures, cumulative, inputs = memory_states(
        keys, values, columns[2], forget_bias, forget_shift
    )
    others = columns[3:]
    queries = others[0].astype(jnp.bfloat16)
    outgates = others[1].astype(jnp.bfloat16)
    exit_rows = others[2].astype(jnp.bfloat16)
    entry_rows = others[3].astype(jnp.bfloat16)
    signal_rows = others[4].astype(jnp.bfloat16)
    mixed_in = (entry_rows.astype(jnp.float32) * signal_rows.astype(jnp.float32)).astype(
        jnp.bfloat16
    )
    rim = passed_along(mixed_in[count - (KERNEL - 1) :], "sp", 1)
    padded = jnp.concatenate([rim, mixed_in], axis=0).astype(jnp.float32)
    response = conv_kernel[0] * padded[0:count]
    for tap in range(1, KERNEL):
        response = response + conv_kernel[tap] * padded[tap : tap + count]
    conv_out = (exit_rows.astype(jnp.float32) * response).astype(jnp.bfloat16)
    memory_out = memory_output(
        queries, keys, values, outgates, inputs, cumulative, gate_apertures, head_norm_gain
    )
    memory_all, conv_all = (
        lax.all_gather(memory_out, "tp", axis=1, tiled=True),
        lax.all_gather(conv_out, "tp", axis=1, tiled=True),
    )
    concatenated_result = jnp.concatenate([memory_all, conv_all], axis=1)
    mixed = add_product(
        concatenated_result, lax.all_gather(merge_weight, ("sp", "fs"), axis=0, tiled=True)
    )
    return mixed.astype(jnp.bfloat16)[None]


def whole_states(keys, values, inputs, logs, blocks):
    heads = inputs.shape[1]
    inputs = inputs.reshape(blocks, BLOCK, heads)
    upto = jnp.tril(jnp.ones((BLOCK, BLOCK), jnp.float32))
    cumulative = jnp.einsum(
        "js,csh->cjh", upto, logs.reshape(blocks, BLOCK, heads), precision=HIGHEST
    )
    last = cumulative[:, -1]
    weight_logs = last[:, None, :] - cumulative + inputs
    peak = jnp.max(weight_logs, axis=1)
    coefficients = jnp.exp(weight_logs - peak[:, None, :])
    scaled = keys.reshape(blocks, BLOCK, heads, DK).astype(jnp.float32) * DK ** (-0.5)
    weighted_keys = scaled * coefficients[..., None]
    value_float = values.reshape(blocks, BLOCK, heads, DV).astype(jnp.float32)
    states = jnp.einsum("cshk,cshv->chkv", weighted_keys, value_float, precision=HIGHEST)
    place = jnp.arange(blocks)
    between = (place[None, :, None] < place[None, None, :]) & (
        place[None, None, :] < place[:, None, None]
    )
    decay = jnp.sum(jnp.where(between[..., None], last[None, None], 0.0), axis=2) + peak[None]
    earlier = (place[None, :] < place[:, None])[..., None]
    decay = jnp.where(earlier, decay, -jnp.inf)
    start = jnp.sum(jnp.where(earlier, last[None], 0.0), axis=1)
    ceiling = jnp.maximum(start, jnp.max(decay, axis=1))
    shares = jnp.exp(decay - ceiling[:, None])
    before = jnp.einsum("cdh,dhkv->chkv", shares, states, precision=HIGHEST)
    return ((before, ceiling), cumulative, inputs)


def resharded(
    tokens,
    norm_gain,
    query_weight,
    key_weight,
    value_weight,
    outgate_weight,
    gate_weight,
    forget_bias,
    forget_shift,
    head_norm_gain,
    exit_weight,
    entry_weight,
    signal_weight,
    conv_kernel,
    merge_weight,
):
    parts = lax.axis_size("sp")
    place = lax.axis_index("sp")
    depth = key_weight.shape[0]
    gates = gate_weight.shape[2]
    heads = gates // parts
    stack = [
        query_weight,
        key_weight,
        value_weight,
        outgate_weight,
        exit_weight,
        entry_weight,
        signal_weight,
        gate_weight.reshape(depth, 2, parts, heads).transpose(0, 2, 1, 3),
    ]
    stacked = jnp.concatenate([w.reshape(depth, parts, -1) for w in stack], axis=2)
    widths = [w.size // depth // parts for w in stack]
    sent = lax.all_to_all(stacked.transpose(1, 0, 2), "sp", 0, 0)
    rows = lax.all_gather(sent, "fs", axis=1)
    rows = rows.reshape(-1, rows.shape[-1])
    line = lax.all_gather(tokens[0], "sp", axis=0, tiled=True)
    whole = lax.all_gather(line, "tp", axis=1, tiled=True)
    count = whole.shape[0]
    flat = whole.astype(jnp.float32)
    normed = (
        flat * lax.rsqrt(jnp.mean(flat * flat, axis=-1, keepdims=True) + EPSILON) * norm_gain
    ).astype(jnp.bfloat16)
    total = add_product(normed, rows)
    columns = []
    offset = 0
    for width in widths:
        columns.append(total[:, offset : offset + width])
        offset = offset + width
    queries, keys, values, outgates, exit_rows, entry_rows, signal_rows = [
        c.astype(jnp.bfloat16) for c in columns[:7]
    ]
    gate_pre = columns[7]

    def own(array, axis, width):
        return lax.dynamic_slice_in_dim(array, place * width, width, axis)

    shift = lax.all_to_all(forget_shift[0].reshape(parts, heads, -1), "sp", 0, 0)
    shift = shift.transpose(1, 0, 2).reshape(heads, count)
    logs = jax.nn.log_sigmoid(gate_pre[:, heads:] + own(forget_bias, 0, heads)) + shift.T
    blocks = count // BLOCK
    apertures, cumulative, inputs = whole_states(keys, values, gate_pre[:, :heads], logs, blocks)
    channels = exit_rows.shape[1]
    taps = own(conv_kernel, 1, channels)
    mixed_in = (entry_rows.astype(jnp.float32) * signal_rows.astype(jnp.float32)).astype(
        jnp.bfloat16
    )
    padded = jnp.pad(mixed_in, ((KERNEL - 1, 0), (0, 0))).astype(jnp.float32)
    response = taps[0] * padded[0:count]
    for tap in range(1, KERNEL):
        response = response + taps[tap] * padded[tap : tap + count]
    conv_out = (exit_rows.astype(jnp.float32) * response).astype(jnp.bfloat16)
    memory_out = memory_output(
        queries,
        keys,
        values,
        outgates,
        inputs,
        cumulative,
        apertures,
        own(head_norm_gain, 0, heads * DV),
    )
    both = jnp.concatenate([memory_out, conv_out], axis=1)
    back = lax.all_to_all(both.reshape(parts, count // parts, -1), "sp", 0, 0)
    halves = lax.all_gather(back, "tp")
    memory_width = heads * DV
    memory_all = halves[..., :memory_width].transpose(2, 0, 1, 3).reshape(count // parts, -1)
    conv_all = halves[..., memory_width:].transpose(2, 0, 1, 3).reshape(count // parts, -1)
    merge = lax.all_gather(merge_weight, ("sp", "fs"), axis=0, tiled=True)
    mixed = add_product(jnp.concatenate([memory_all, conv_all], axis=1), merge)
    return mixed.astype(jnp.bfloat16)[None]


def solution(mesh):
    placed = (
        P("fs", "sp", "tp"),
        P(),
        P(("sp", "fs"), "tp"),
        P(("sp", "fs"), "tp"),
        P(("sp", "fs"), "tp"),
        P(("sp", "fs"), "tp"),
        P(("sp", "fs"), None, "tp"),
        P("tp"),
        P("fs", "tp", "sp"),
        P("tp"),
        P(("sp", "fs"), "tp"),
        P(("sp", "fs"), "tp"),
        P(("sp", "fs"), "tp"),
        P(None, "tp"),
        P(("sp", "fs"), "tp"),
    )
    sp, tp = (mesh.shape["sp"], mesh.shape["tp"])

    def step(*args):
        heads, channels = (args[6].shape[2], args[10].shape[1])
        even = heads % (sp * tp) == 0 and channels % (sp * tp * 128) == 0
        body = resharded if even else local
        return jax.shard_map(
            body, mesh=mesh, in_specs=placed, out_specs=P("fs", "sp", "tp"), check_vma=False
        )(*args)

    return step
```

profile of v0, /device:TPU:0, one launch (start us, length us, event | category | flops | bytes accessed | tf_op | source)
XLA Modules:
  0.0 471.0 jit_solution(17754036155125778785)
XLA Ops:
  7.3 1.0 copy.151
  8.3 1.0 copy.152
  9.4 1.1 copy.153
  11.6 85.0 %all_to_all.15 = bf16[4,128,1540]{1,2,0:T(8,128)(2,1)} all-to-all(bf16[4,128,1540]{1,2,0:T(8,128)(2,1)S(1)} %bitcast.143), channel_id=1, replica_groups=mesh['sp'=4,'fs'=4,'tp'=2] {'sp'}, dimensions={0} | all-to-all | bytes 3153920 | tf_op jit(solution)/shard_map/all_to_all | solution.py:264
  96.6 26.0 %all-gather.12.cloned.1.call-done = bf16[1,2048,1024]{2,1,0:T(8,128)(2,1)} async-done(((bf16[1,512,1024]{2,1,0:T(8,128)(2,1)}), bf16[1,2048,1024]{2,1,0:T(8,128)(2,1)}) %all-gather.12.cloned.1.call-update) | async-done | bytes 4194320 | tf_op jit(solution)/shard_map/all_gather | solution.py:267
  123.9 3.3 all-to-all-start.1
  129.0 64.8 %all-gather.16.cloned.1.call-done = bf16[4,512,1540]{1,2,0:T(8,128)(2,1)} async-done(((bf16[4,128,1540]{1,2,0:T(8,128)(2,1)}), bf16[4,512,1540]{1,2,0:T(8,128)(2,1)}) %all-gather.16.cloned.1.call-update) | async-done | bytes 6307856 | tf_op jit(solution)/shard_map/all_gather | solution.py:265
  193.9 17.7 %copy.243 = bf16[4,512,1540]{1,0,2:T(4,128)(2,1)S(1)} copy(bf16[4,512,1540]{1,2,0:T(8,128)(2,1)} %all-gather.16.cloned.1.call-done) | data formatting | bytes 12615680 | tf_op jit(solution)/shard_map/all_gather | solution.py:265
  211.6 2.6 pad.9
  214.2 5.3 %copy.191 = bf16[193,8,4,512]{3,1,2,0:T(8,128)(2,1)} copy(bf16[193,8,4,512]{3,2,1,0:T(4,128)(2,1)S(1)} %bitcast.129) | data formatting | bytes 12648448
  219.5 5.2 %fusion = f32[2048]{0:T(1024)S(1)} fusion(bf16[1,2048,2048]{2,1,0:T(8,128)(2,1)} %all-gather.14.cloned.1.call-done), kind=kLoop, calls=%fused_computation.2 | loop fusion | flops 12580864 | bytes 8396800 | tf_op jit(solution)/shard_map/reduce_sum | solution.py:272
  225.3 18.9 %fusion.78 = (bf16[2048,1540]{0,1:T(8,128)(2,1)}, f32[2048,1540]{0,1:T(8,128)}) fusion(bf16[2048,1540]{0,1:T(8,128)(2,1)} %bitcast.135, bf16[1,2048,2048]{2,1,0:T(8,128)(2,1)S(1)} %copy-done, f32[2048]{0:T(1024)S(1)} %copy-done.9, f32[2048]{0:T(1024)S(1)} %add_rsqrt_fusion), kind=kOutput, calls=%fused_computation.117 | convolution fusion | flops 12938387456 | bytes 33636352 | tf_op jit(solution)/shard_map/dot_general | solution.py:51
  244.1 1.0 fusion.56
  246.3 1.3 fusion.20
  247.8 1.3 slice_bitcast_fusion.2
  249.1 1.3 slice_bitcast_fusion
  250.8 0.9 copy.177
  251.7 1.0 fusion.31
  252.7 1.6 convolution_bitcast_fusion
  255.3 1.9 fusion.28
  257.2 4.6 multiply_reduce_fusion
  261.8 2.1 fusion.19
  264.0 1.2 copy.183
  265.2 3.3 fusion.13
  268.9 2.7 fusion.16
  272.1 52.4 %all_to_all.16 = bf16[4,512,512]{1,2,0:T(8,128)(2,1)S(1)} all-to-all(bf16[4,512,512]{1,2,0:T(8,128)(2,1)S(1)} %bitcast.133), channel_id=1, replica_groups=mesh['sp'=4,'fs'=4,'tp'=2] {'sp'}, dimensions={0} | all-to-all | bytes 4194304 | tf_op jit(solution)/shard_map/all_to_all | solution.py:314
  324.5 2.4 copy.185
  327.5 11.4 %all-gather.18.cloned.1.call-done = bf16[8,512,512]{2,1,0:T(8,128)(2,1)} async-done(((bf16[4,512,512]{2,1,0:T(8,128)(2,1)}), bf16[8,512,512]{2,1,0:T(8,128)(2,1)}) %all-gather.18.cloned.1.call-update) | async-done | bytes 4194320 | tf_op jit(solution)/shard_map/all_gather | solution.py:315
  338.9 6.4 %copy.186 = bf16[8,512,512]{1,2,0:T(8,128)(2,1)} copy(bf16[8,512,512]{2,1,0:T(8,128)(2,1)} %all-gather.18.cloned.1.call-done) | data formatting | bytes 8388608 | tf_op jit(solution)/shard_map/all_gather | solution.py:315
  345.3 4.0 fusion.77
  349.3 105.7 %all-gather.10.cloned.1.call-done = bf16[4096,1024]{1,0:T(8,128)(2,1)} async-done(((bf16[256,1024]{1,0:T(8,128)(2,1)}), bf16[4096,1024]{1,0:T(8,128)(2,1)}) %all-gather.10.cloned.1.call-update) | async-done | bytes 8388624 | tf_op jit(solution)/shard_map/all_gather | solution.py:319
  455.0 9.5 %fusion.25 = bf16[1,512,1024]{2,1,0:T(8,128)(2,1)} fusion(bf16[4096,1024]{1,0:T(8,128)(2,1)} %all-gather.10.cloned.1.call-done, bf16[512,2048]{0,1:T(8,128)(2,1)} %bitcast.142, bf16[512,2048]{0,1:T(8,128)(2,1)S(1)} %bitcast.141), kind=kOutput, calls=%fused_computation.36 | convolution fusion | flops 4303880192 | bytes 13631488 | tf_op jit(solution)/shard_map/dot_general | solution.py:51
  (80 shorter events, 9.4 us)
Async XLA Ops:
  6.5 4.0 copy-start.3
  6.5 4.2 copy-start.4
  6.5 4.3 copy-start.5
  6.5 4.5 copy-start.6
  6.5 116.0 %all-gather.12.cloned.1.call-start = ((), (), s32[]{:S(2)}) async-start(), calls=%async_computation.4 | async-start | bytes 5242880 | tf_op jit(solution)/shard_map/all_gather | solution.py:267
  6.6 4.7 copy-start.8
  7.3 186.6 %all-gather.16.cloned.1.call-start = ((), (), s32[]{:S(2)}) async-start(), calls=%async_computation.6 | async-start | bytes 7905280 | tf_op jit(solution)/shard_map/all_gather | solution.py:265
  96.5 123.0 %all-gather.14.cloned.1.call-start = ((), (), s32[]{:S(2)}) async-start(), calls=%async_computation.5 | async-start | bytes 12582912 | tf_op jit(solution)/shard_map/all_gather | solution.py:268
  122.6 0.7 copy-start.7
  122.6 4.7 copy-start.10
  123.9 120.2 %all-to-all-start.1 = ((f32[4,2,512]{2,1,0:T(2,128)}), f32[4,2,512]{2,1,0:T(2,128)S(1)}, u32[]{:S(2)}, u32[]{:S(2)}) async-start(f32[4,2,512]{2,1,0:T(2,128)} %reshape_squeeze.3), calls=%async_computation.1 | async-start | bytes 32768 | tf_op jit(solution)/shard_map/all_to_all | solution.py:288
  127.2 211.7 %all-gather.18.cloned.1.call-start = ((), (), s32[]{:S(2)}) async-start(), calls=%async_computation.7 | async-start | bytes 6291456 | tf_op jit(solution)/shard_map/all_gather | solution.py:315
  219.5 5.3 %copy-start.9 = (f32[2048]{0:T(1024)S(1)}, f32[2048]{0:T(1024)}, u32[]{:S(2)}) copy-start(f32[2048]{0:T(1024)} %param.16) | copy-start | bytes 24580
  219.5 5.8 %copy-start = (bf16[1,2048,2048]{2,1,0:T(8,128)(2,1)S(1)}, bf16[1,2048,2048]{2,1,0:T(8,128)(2,1)}, u32[]{:S(2)}) copy-start(bf16[1,2048,2048]{2,1,0:T(8,128)(2,1)} %all-gather.14.cloned.1.call-done) | copy-start | bytes 25165828
  250.6 1.2 copy-start.1
  254.4 0.8 copy-start.2
  326.9 128.1 %all-gather.10.cloned.1.call-start = ((), (), s32[]{:S(2)}) async-start(), calls=%async_computation.3 | async-start | bytes 8912896 | tf_op jit(solution)/shard_map/all_gather | solution.py:319
Sparse Core Ops, SparseCore 0:
  8.9 113.6 all-gather.11
  124.4 69.3 all-gather.15
  195.4 19.8 all-gather.13
  327.0 11.7 all-gather.17
  341.5 113.4 all-gather.9
where the time goes:
time: 472 us; the launch traced here: 471 us
  waiting for transfers between devices  209 us (44%)
  blocking collectives  137 us (29%)
  local copies, waits for them, and re-layouts  52.9 us (11%)
  matrix products  37.7 us (8%)
  other arithmetic  16.9 us (4%)
  between operations  13.6 us (3%)
    all_gather x1, waiting for transfers between devices, resharded(): merge = lax.all_gather(merge_weight, ('sp', 'fs'), axis=0, tiled=True)  106 us
    all_to_all x1, blocking collectives, resharded(): sent = lax.all_to_all(stacked.transpose(1, 0, 2), 'sp', 0, 0)  85 us
    all_gather x1, waiting for transfers between devices, resharded(): rows = lax.all_gather(sent, 'fs', axis=1)  64.8 us
    all_to_all x1, blocking collectives, resharded(): back = lax.all_to_all(both.reshape(parts, count // parts, -1), 'sp', 0, 0)  52.4 us
    dot_general x2, matrix products, add_product(): return jnp.dot(left, piece, preferred_element_type=jnp.float32)  28.4 us
    all_gather x1, waiting for transfers between devices, resharded(): line = lax.all_gather(tokens[0], 'sp', axis=0, tiled=True)  26 us
    all_gather x1, local copies, waits for them, and re-layouts, resharded(): rows = lax.all_gather(sent, 'fs', axis=1)  17.7 us
    unnamed x46, local copies, waits for them, and re-layouts  17.2 us
  transfers between devices with their start and end apart: 6, of which 4 were waited for; matrix products, arithmetic and copies ran while one was open for 14% of the time, Pallas kernels for 0%

commit v1 on v0

--- a/solution.py
+++ b/solution.py
@@ -265,7 +265,7 @@
     rows = lax.all_gather(sent, "fs", axis=1)
     rows = rows.reshape(-1, rows.shape[-1])
     line = lax.all_gather(tokens[0], "sp", axis=0, tiled=True)
-    whole = lax.all_gather(line, "tp", axis=1, tiled=True)
+    whole = jnp.concatenate(lax.all_gather(line, "tp"), axis=1)
     count = whole.shape[0]
     flat = whole.astype(jnp.float32)
     normed = (

time: 472 us -> 494 us (1.047)
  local copies, waits for them, and re-layouts: 52.9 us -> 64.4 us
  other arithmetic: 16.9 us -> 25.3 us
    all_gather x0 -> x1, local copies, waits for them, and re-layouts: none -> 11.7 us  [resharded(): whole = jnp.concatenate(lax.all_gather(line, 'tp'), axis=1)]
    convert_element_type x0 -> x1, other arithmetic: none -> 8.55 us  [resharded(): normed = (flat * lax.rsqrt(jnp.mean(flat * flat, axis=-1, keepdims=True)...]
    unnamed x46 -> x44, local copies, waits for them, and re-layouts: 17.2 us -> 16.7 us
  transfers between devices with their start and end apart: 6 -> 6, of which waited for: 4 -> 4; matrix products, arithmetic and copies ran while one was open for 14% -> 18% of each run, Pallas kernels for 0% -> 0%
where the time goes in v1:
time: 494 us; the launch traced here: 492 us
  waiting for transfers between devices  209 us (42%)
  blocking collectives  137 us (28%)
  local copies, waits for them, and re-layouts  64.4 us (13%)
  matrix products  39.2 us (8%)
  other arithmetic  25.3 us (5%)
  between operations  13.6 us (3%)
    all_gather x1, waiting for transfers between devices, resharded(): merge = lax.all_gather(merge_weight, ('sp', 'fs'), axis=0, tiled=True)  106 us
    all_to_all x1, blocking collectives, resharded(): sent = lax.all_to_all(stacked.transpose(1, 0, 2), 'sp', 0, 0)  85 us
    all_gather x1, waiting for transfers between devices, resharded(): rows = lax.all_gather(sent, 'fs', axis=1)  64.8 us
    all_to_all x1, blocking collectives, resharded(): back = lax.all_to_all(both.reshape(parts, count // parts, -1), 'sp', 0, 0)  52.4 us
    dot_general x2, matrix products, add_product(): return jnp.dot(left, piece, preferred_element_type=jnp.float32)  29.9 us
    all_gather x1, waiting for transfers between devices, resharded(): line = lax.all_gather(tokens[0], 'sp', axis=0, tiled=True)  26 us
    all_gather x1, local copies, waits for them, and re-layouts, resharded(): rows = lax.all_gather(sent, 'fs', axis=1)  17.7 us
    unnamed x44, local copies, waits for them, and re-layouts  16.7 us
  transfers between devices with their start and end apart: 6, of which 4 were waited for; matrix products, arithmetic and copies ran while one was open for 18% of the time, Pallas kernels for 0%

profile of v1, /device:TPU:0, one launch (start us, length us, event | category | flops | bytes accessed | tf_op | source)
XLA Modules:
  0.0 492.5 jit_solution(5456183551933837473)
XLA Ops:
  8.3 1.0 copy.157
  9.4 1.1 copy.158
  11.6 85.0 %all_to_all.15 = bf16[4,128,1540]{1,2,0:T(8,128)(2,1)} all-to-all(bf16[4,128,1540]{1,2,0:T(8,128)(2,1)S(1)} %bitcast.139), channel_id=1, replica_groups=mesh['sp'=4,'fs'=4,'tp'=2] {'sp'}, dimensions={0} | all-to-all | bytes 3153920 | tf_op jit(solution)/shard_map/all_to_all | solution.py:264
  96.6 26.0 %all-gather.12.cloned.1.call-done = bf16[1,2048,1024]{2,1,0:T(8,128)(2,1)} async-done(((bf16[1,512,1024]{2,1,0:T(8,128)(2,1)}), bf16[1,2048,1024]{2,1,0:T(8,128)(2,1)}) %all-gather.12.cloned.1.call-update) | async-done | bytes 4194320 | tf_op jit(solution)/shard_map/all_gather | solution.py:267
  123.9 3.3 all-to-all-start.1
  129.1 64.8 %all-gather.16.cloned.1.call-done = bf16[4,512,1540]{1,2,0:T(8,128)(2,1)} async-done(((bf16[4,128,1540]{1,2,0:T(8,128)(2,1)}), bf16[4,512,1540]{1,2,0:T(8,128)(2,1)}) %all-gather.16.cloned.1.call-update) | async-done | bytes 6307856 | tf_op jit(solution)/shard_map/all_gather | solution.py:265
  193.9 17.7 %copy.248 = bf16[4,512,1540]{1,0,2:T(4,128)(2,1)S(1)} copy(bf16[4,512,1540]{1,2,0:T(8,128)(2,1)} %all-gather.16.cloned.1.call-done) | data formatting | bytes 12615680 | tf_op jit(solution)/shard_map/all_gather | solution.py:265
  211.6 2.6 pad.9
  214.2 5.4 %copy.196 = bf16[193,8,4,512]{3,1,2,0:T(8,128)(2,1)} copy(bf16[193,8,4,512]{3,2,1,0:T(4,128)(2,1)S(1)} %bitcast.124) | data formatting | bytes 12648448
  219.5 11.7 %copy.155 = bf16[2,2048,1024]{1,2,0:T(8,128)(2,1)} copy(bf16[2,2048,1024]{2,1,0:T(8,128)(2,1)} %all-gather.14.cloned.1.call-done) | data formatting | bytes 16777216 | tf_op jit(solution)/shard_map/all_gather | solution.py:268
  231.3 5.1 %fusion = f32[2048]{0:T(1024)S(1)} fusion(bf16[2,2048,1024]{1,2,0:T(8,128)(2,1)} %copy.155), kind=kLoop, calls=%fused_computation.2 | loop fusion | flops 12580864 | bytes 8396800 | tf_op jit(solution)/shard_map/reduce_sum | solution.py:272
  236.4 8.6 %fusion.2 = bf16[2,2048,1024]{1,2,0:T(8,128)(2,1)} fusion(bf16[2,2048,1024]{1,2,0:T(8,128)(2,1)} %copy.155, f32[2,1024]{1,0:T(2,128)S(1)} %mul.132, f32[2048]{0:T(1024)S(1)} %add_rsqrt_fusion), kind=kLoop, calls=%fused_computation.4 | loop fusion | flops 16777216 | bytes 16793600 | tf_op jit(solution)/shard_map/convert_element_type | solution.py:273
  244.9 20.4 %fusion.73 = (bf16[2048,1540]{0,1:T(8,128)(2,1)}, f32[2048,1540]{0,1:T(8,128)}) fusion(bf16[2048,2048]{0,1:T(8,128)(2,1)} %bitcast.127, bf16[2048,1540]{0,1:T(8,128)(2,1)} %bitcast.131), kind=kOutput, calls=%fused_computation.113 | convolution fusion | flops 12921610240 | bytes 33619968 | tf_op jit(solution)/shard_map/dot_general | solution.py:51
  265.3 1.0 fusion.51
  267.5 1.3 fusion.15
  269.0 1.3 slice_bitcast_fusion.2
  270.3 1.3 slice_bitcast_fusion
  272.0 1.1 copy.182
  274.1 1.6 convolution_bitcast_fusion
  276.7 1.9 fusion.23
  278.6 4.6 multiply_reduce_fusion
  283.2 2.1 fusion.14
  285.4 1.2 copy.188
  286.6 3.3 fusion.8
  290.3 2.7 fusion.11
  293.5 52.4 %all_to_all.16 = bf16[4,512,512]{1,2,0:T(8,128)(2,1)S(1)} all-to-all(bf16[4,512,512]{1,2,0:T(8,128)(2,1)S(1)} %bitcast.129), channel_id=1, replica_groups=mesh['sp'=4,'fs'=4,'tp'=2] {'sp'}, dimensions={0} | all-to-all | bytes 4194304 | tf_op jit(solution)/shard_map/all_to_all | solution.py:314
  346.0 2.4 copy.190
  349.0 11.4 %all-gather.18.cloned.1.call-done = bf16[8,512,512]{2,1,0:T(8,128)(2,1)} async-done(((bf16[4,512,512]{2,1,0:T(8,128)(2,1)}), bf16[8,512,512]{2,1,0:T(8,128)(2,1)}) %all-gather.18.cloned.1.call-update) | async-done | bytes 4194320 | tf_op jit(solution)/shard_map/all_gather | solution.py:315
  360.3 6.5 %copy.191 = bf16[8,512,512]{1,2,0:T(8,128)(2,1)} copy(bf16[8,512,512]{2,1,0:T(8,128)(2,1)} %all-gather.18.cloned.1.call-done) | data formatting | bytes 8388608 | tf_op jit(solution)/shard_map/all_gather | solution.py:315
  366.8 4.0 fusion.72
  370.8 105.7 %all-gather.10.cloned.1.call-done = bf16[4096,1024]{1,0:T(8,128)(2,1)} async-done(((bf16[256,1024]{1,0:T(8,128)(2,1)}), bf16[4096,1024]{1,0:T(8,128)(2,1)}) %all-gather.10.cloned.1.call-update) | async-done | bytes 8388624 | tf_op jit(solution)/shard_map/all_gather | solution.py:319
  476.4 9.5 %fusion.20 = bf16[1,512,1024]{2,1,0:T(8,128)(2,1)} fusion(bf16[4096,1024]{1,0:T(8,128)(2,1)} %all-gather.10.cloned.1.call-done, bf16[512,2048]{0,1:T(8,128)(2,1)} %bitcast.138, bf16[512,2048]{0,1:T(8,128)(2,1)S(1)} %bitcast.137), kind=kOutput, calls=%fused_computation.32 | convolution fusion | flops 4303880192 | bytes 13631488 | tf_op jit(solution)/shard_map/dot_general | solution.py:51
  (81 shorter events, 10.9 us)
Async XLA Ops:
  6.5 4.0 copy-start.2
  6.5 4.2 copy-start.3
  6.5 4.3 copy-start.4
  6.5 4.5 copy-start.5
  6.5 116.0 %all-gather.12.cloned.1.call-start = ((), (), s32[]{:S(2)}) async-start(), calls=%async_computation.4 | async-start | bytes 5242880 | tf_op jit(solution)/shard_map/all_gather | solution.py:267
  6.6 4.7 copy-start.8
  7.3 186.6 %all-gather.16.cloned.1.call-start = ((), (), s32[]{:S(2)}) async-start(), calls=%async_computation.6 | async-start | bytes 7905280 | tf_op jit(solution)/shard_map/all_gather | solution.py:265
  96.5 123.0 %all-gather.14.cloned.1.call-start = ((), (), s32[]{:S(2)}) async-start(), calls=%async_computation.5 | async-start | bytes 12582912 | tf_op jit(solution)/shard_map/all_gather | solution.py:268
  122.6 0.7 copy-start.6
  122.6 4.7 copy-start.7
  122.6 4.7 copy-start.9
  123.9 141.4 %all-to-all-start.1 = ((f32[4,2,512]{2,1,0:T(2,128)}), f32[4,2,512]{2,1,0:T(2,128)S(1)}, u32[]{:S(2)}, u32[]{:S(2)}) async-start(f32[4,2,512]{2,1,0:T(2,128)} %reshape_squeeze.3), calls=%async_computation.1 | async-start | bytes 32768 | tf_op jit(solution)/shard_map/all_to_all | solution.py:288
  127.2 233.1 %all-gather.18.cloned.1.call-start = ((), (), s32[]{:S(2)}) async-start(), calls=%async_computation.7 | async-start | bytes 6291456 | tf_op jit(solution)/shard_map/all_gather | solution.py:315
  271.8 1.4 copy-start
  275.9 0.8 copy-start.1
  348.4 128.1 %all-gather.10.cloned.1.call-start = ((), (), s32[]{:S(2)}) async-start(), calls=%async_computation.3 | async-start | bytes 8912896 | tf_op jit(solution)/shard_map/all_gather | solution.py:319
Sparse Core Ops, SparseCore 0:
  8.9 113.6 all-gather.11
  124.4 69.3 all-gather.15
  195.4 19.8 all-gather.13
  348.5 11.7 all-gather.17
  362.9 113.4 all-gather.9
